TPU v7x, 256 devices: a whole 4x4x8 slice. The times are simulated.
256 devices in a mesh: ep: 16 (over y, x), tp: 16 (over z, core).
Axes of the slice: x: 4, y: 4, z: 8, core: 2. Of those that a mesh axis runs over, the one named last changes fastest.
Arguments:
- query_latent: bfloat16 [8192, 1024], P('ep'), may hold values from -6 to 6
- joint_latent: bfloat16 [8192, 512], P('ep'), may hold values from -6 to 6
- rotary_key: bfloat16 [8192, 32], P('ep'), may hold values from -60 to 60
- query_gain: float32 [1024], replicated, may hold values from 0.1 to 1.9
- joint_gain: float32 [512], replicated, may hold values from 0.1 to 1.9
- query_weight: bfloat16 [1024, 2048], P(None, 'tp'), may hold values from -0.1875 to 0.1875
- query_rotary: bfloat16 [1024, 1024], P(None, 'tp'), may hold values from -0.1875 to 0.1875
- key_weight: bfloat16 [512, 2048], P(None, 'tp'), may hold values from -0.25 to 0.25
- value_weight: bfloat16 [512, 2048], P(None, 'tp'), may hold values from -0.25 to 0.25
- output_weight: bfloat16 [2048, 2048], P('tp'), may hold values from -6 to 6
- expert_input: bfloat16 [8192, 2048], P('ep'), may hold values from -6 to 6
- expert_gain: float32 [2048], replicated, may hold values from 0.1 to 1.9
- routes: int32 [8192, 2], P('ep'), may hold values from 0 to 31, all different within a row; in each aligned block of 512 rows (0 to 511, 512 to 1023, ...) at most 48 rows name the same one
- route_weight: float32 [8192, 2], P('ep'), may hold values from 0.2 to 1
- gate_weight: bfloat16 [32, 2048, 4096], P('ep', None, 'tp'), may hold values from -0.125 to 0.125
- up_weight: bfloat16 [32, 2048, 4096], P('ep', None, 'tp'), may hold values from -0.125 to 0.125
- down_weight: bfloat16 [32, 4096, 2048], P('ep', 'tp'), may hold values from -0.09375 to 0.09375
Outputs:
- mixer_out: bfloat16 [8192, 2048], P(('ep', 'tp'))
- expert_out: bfloat16 [8192, 2048], P('ep', 'tp')
Inputs may be any that keep to these rules, and one draw needn't show every extreme that they name: `routes`: A row names 2 different experts. Among the rows of one device (aligned blocks of 512 rows) no expert is named by more than 48 rows, a bound that some block reaches.
All inputs are finite; a program needn't handle non-finite values.
Results may differ from a plain program's by a relative error of at most 0.019.
The roundings to bfloat16 on the way count: a program that leaves them out, or rounds other values in their place, can miss the bound.
Values may be sent and summed in bfloat16 or wider, within the bound.
A program may use at most 128 MiB of HBM per device.

v0:
```python
import jax
import jax.numpy as jnp
from jax import lax
from jax.sharding import PartitionSpec as P

NOPE = 64
VDIM = 64
NORM_EPSILON = 1e-06
ROTARY_BASE = 10000.0


def sent_together(arrays, axis, dim, along):
    both = jnp.concatenate(arrays, axis=along)
    out, at, outs = (lax.all_gather(both, axis, axis=dim, tiled=True), 0, [])
    for a in arrays:
        outs.append(lax.slice_in_dim(out, at, at + a.shape[along], axis=along))
        at += a.shape[along]
    return tuple(outs)


def norm_rows(source, gain_vector):
    as_float = source.astype(jnp.float32)
    factor = lax.rsqrt(jnp.mean(as_float * as_float, axis=-1, keepdims=True) + NORM_EPSILON)
    return (as_float * factor * gain_vector).astype(jnp.bfloat16)


def rotate(source, positions):
    half_width = source.shape[-1] // 2
    frequencies = ROTARY_BASE ** (-jnp.arange(half_width, dtype=jnp.float32) / half_width)
    angles = positions[:, None] * frequencies[None, :]
    view_shape = (source.shape[0],) + (1,) * (source.ndim - 2) + (half_width,)
    cosine_table = jnp.cos(angles).reshape(view_shape)
    sine_table = jnp.sin(angles).reshape(view_shape)
    first_half = source[..., :half_width]
    second = source[..., half_width:]
    return jnp.concatenate(
        [
            first_half * cosine_table - second * sine_table,
            second * cosine_table + first_half * sine_table,
        ],
        axis=-1,
    )


def attend_block(
    carried, query_plain, query_turned, key_block, value_block, turned_block, score_scale
):
    row_top, row_total, mixed_values = carried
    scores = jnp.einsum("qhd,khd->qhk", query_plain, key_block, preferred_element_type=jnp.float32)
    scores = scores + jnp.einsum(
        "qhd,kd->qhk", query_turned, turned_block, preferred_element_type=jnp.float32
    )
    scores = scores * score_scale
    new_top = jnp.maximum(row_top, jnp.max(scores, axis=-1))
    factor = jnp.exp(row_top - new_top)
    expo = jnp.exp(scores - new_top[..., None])
    row_total = row_total * factor + jnp.sum(expo, axis=-1)
    mixed_values = mixed_values * factor[..., None] + jnp.einsum(
        "qhk,khd->qhd", expo.astype(jnp.bfloat16), value_block, preferred_element_type=jnp.float32
    )
    return (new_top, row_total, mixed_values)


def token_mixer(
    query_latent,
    joint_latent,
    rotary_key,
    query_gain,
    joint_gain,
    query_weight,
    query_rotary,
    key_weight,
    value_weight,
    output_weight,
):
    row_count = query_latent.shape[0]
    head_count = key_weight.shape[1] // NOPE
    turn_width = rotary_key.shape[1]
    offset = lax.axis_index("ep") * row_count
    positions = (offset + jnp.arange(row_count, dtype=jnp.int32)).astype(jnp.float32)
    query_normed = norm_rows(query_latent, query_gain)
    joint_normed = norm_rows(joint_latent, joint_gain)
    turned_key = rotate(rotary_key.astype(jnp.float32), positions).astype(jnp.bfloat16)
    query_plain = jnp.dot(query_normed, query_weight, preferred_element_type=jnp.float32).astype(
        jnp.bfloat16
    )
    query_plain = query_plain.reshape(row_count, head_count, NOPE)
    query_turned = jnp.dot(query_normed, query_rotary, preferred_element_type=jnp.float32)
    query_turned = rotate(
        query_turned.reshape(row_count, head_count, turn_width), positions
    ).astype(jnp.bfloat16)
    score_scale = (NOPE + turn_width) ** (-0.5)
    start_carry = (
        jnp.full((row_count, head_count), -jnp.inf, jnp.float32),
        jnp.zeros((row_count, head_count), jnp.float32),
        jnp.zeros((row_count, head_count, VDIM), jnp.float32),
    )
    carried = start_carry
    latent_piece, turned_piece = sent_together((joint_normed, turned_key), "ep", 0, 1)
    block_rows = min(row_count, latent_piece.shape[0])
    block_total = latent_piece.shape[0] // block_rows

    def scan_step(inner_carry, key_items):
        latent_block, turned_block = key_items
        key_block = jnp.dot(latent_block, key_weight, preferred_element_type=jnp.float32)
        key_block = key_block.astype(jnp.bfloat16).reshape(block_rows, head_count, NOPE)
        value_block = jnp.dot(latent_block, value_weight, preferred_element_type=jnp.float32)
        value_block = value_block.astype(jnp.bfloat16).reshape(block_rows, head_count, VDIM)
        return (
            attend_block(
                inner_carry,
                query_plain,
                query_turned,
                key_block,
                value_block,
                turned_block,
                score_scale,
            ),
            None,
        )

    carried, _ = lax.scan(
        scan_step,
        carried,
        (
            latent_piece.reshape(block_total, block_rows, latent_piece.shape[1]),
            turned_piece.reshape(block_total, block_rows, turn_width),
        ),
    )
    row_top, row_total, mixed_values = carried
    attended = (
        (mixed_values / row_total[..., None])
        .astype(jnp.bfloat16)
        .reshape(row_count, head_count * VDIM)
    )
    return lax.psum_scatter(
        jnp.dot(attended, output_weight, preferred_element_type=jnp.float32).astype(jnp.bfloat16),
        "tp",
        scatter_dimension=0,
        tiled=True,
    )


def experts(expert_input, expert_gain, routes, route_weight, gate_weight, up_weight, down_weight):
    row_count = expert_input.shape[0]
    feature_width = expert_input.shape[1]
    top_count = routes.shape[1]
    group_count = lax.axis_size("ep")
    local_count = gate_weight.shape[0]
    expert_count = local_count * group_count
    capacity = 3 * row_count // (2 * group_count)
    part_width = feature_width // lax.axis_size("tp")
    flat_routes = routes.reshape(-1)
    onehot = (flat_routes[:, None] == jnp.arange(expert_count, dtype=jnp.int32)[None, :]).astype(
        jnp.int32
    )
    rank_within = jnp.sum((jnp.cumsum(onehot, axis=0) - onehot) * onehot, axis=1)
    slot_index = flat_routes * capacity + rank_within
    owner_token = jnp.arange(row_count * top_count, dtype=jnp.int32) // top_count
    slot_token = jnp.zeros((expert_count * capacity,), jnp.int32).at[slot_index].set(owner_token)
    filled = jnp.zeros((expert_count * capacity,), jnp.bfloat16).at[slot_index].set(1.0)
    normed = norm_rows(expert_input, expert_gain)
    columns = lax.dynamic_slice_in_dim(normed, lax.axis_index("tp") * part_width, part_width, 1)
    outgoing = (columns[slot_token] * filled[:, None]).reshape(
        group_count, local_count, capacity, part_width
    )
    arrived = lax.all_to_all(outgoing, "ep", split_axis=0, concat_axis=0, tiled=True)
    piece = lax.all_gather(arrived, "tp", axis=3, tiled=True)
    gate_running = jnp.einsum(
        "secd,edf->secf", piece, gate_weight, preferred_element_type=jnp.float32
    )
    up_running = jnp.einsum("secd,edf->secf", piece, up_weight, preferred_element_type=jnp.float32)
    hidden = (jax.nn.silu(gate_running) * up_running).astype(jnp.bfloat16)
    partial_value = jnp.einsum(
        "secf,efd->secd", hidden, down_weight, preferred_element_type=jnp.float32
    )
    summed = lax.psum_scatter(
        partial_value.astype(jnp.bfloat16), "tp", scatter_dimension=3, tiled=True
    )
    returned = lax.all_to_all(summed, "ep", split_axis=0, concat_axis=0, tiled=True)
    picked = returned.reshape(expert_count * capacity, part_width)[slot_index]
    picked = picked.astype(jnp.float32).reshape(row_count, top_count, part_width)
    return jnp.sum(picked * route_weight[:, :, None], axis=1).astype(jnp.bfloat16)


def local(
    query_latent,
    joint_latent,
    rotary_key,
    query_gain,
    joint_gain,
    query_weight,
    query_rotary,
    key_weight,
    value_weight,
    output_weight,
    expert_input,
    expert_gain,
    routes,
    route_weight,
    gate_weight,
    up_weight,
    down_weight,
):
    mixer_out = token_mixer(
        query_latent,
        joint_latent,
        rotary_key,
        query_gain,
        joint_gain,
        query_weight,
        query_rotary,
        key_weight,
        value_weight,
        output_weight,
    )
    expert_out = experts(
        expert_input, expert_gain, routes, route_weight, gate_weight, up_weight, down_weight
    )
    return (mixer_out, expert_out)


def solution(mesh):
    return jax.shard_map(
        local,
        mesh=mesh,
        in_specs=(
            P("ep", None),
            P("ep", None),
            P("ep", None),
            P(),
            P(),
            P(None, "tp"),
            P(None, "tp"),
            P(None, "tp"),
            P(None, "tp"),
            P("tp", None),
            P("ep", None),
            P(),
            P("ep", None),
            P("ep", None),
            P("ep", None, "tp"),
            P("ep", None, "tp"),
            P("ep", "tp", None),
        ),
        out_specs=(P(("ep", "tp"), None), P("ep", "tp")),
        check_vma=False,
    )
```

profile of v0, /device:TPU:6, one launch (start us, length us, event | category | flops | bytes accessed | tf_op | source)
XLA Modules:
  0.0 353.4 jit_solution(10818710300028206992)
XLA Ops:
  7.2 4.2 %convert_element_type.83 = f32[512,2048]{1,0:T(8,128)} convert(bf16[512,2048]{1,0:T(8,128)(2,1)} %param.29) | non-fusion elementwise | flops 1048576 | bytes 6291456 | tf_op jit(solution)/shard_map/convert_element_type | solution.py:22
  12.7 9.0 %reduce-window.6 = s32[32,8,128]{2,1,0:T(8,128)S(1)} reduce-window(s32[32,8,128]{2,1,0:T(8,128)S(1)} %fusion.46, s32[]{:T(128)} %constant.30.clone.1), window={size=1x1x128 pad=0_0x0_0x127_0}, to_apply=%region_8.9 | reduce-window | flops 4161536 | bytes 262148 | tf_op jit(solution)/shard_map/reduce-window
  22.6 4.3 %scatter_custom_fusion = s32[1536]{0:T(1024)S(1)} fusion(s32[1024]{0:T(1024)S(1)} %bitcast.150, s32[1024]{0:T(1024)S(1)} %add_select_fusion, s32[]{:T(128)} %constant.30.clone.1), kind=kCustom, calls=%fused_computation.89 | custom fusion | bytes 6148 | tf_op jit(solution)/shard_map/scatter | solution.py:160
  26.9 7.6 %scatter_custom_fusion.1 = bf16[1536]{0:T(1024)(128)(2,1)S(1)} fusion(s32[1024]{0:T(1024)S(1)} %bitcast.151, bf16[1024]{0:T(1024)(128)(2,1)S(1)} %broadcast.163, bf16[]{:T(256)} %constant.82.clone.1), kind=kCustom, calls=%fused_computation.93 | custom fusion | bytes 3074 | tf_op jit(solution)/shard_map/scatter | solution.py:161
  36.5 3.2 gather_fusion
  40.0 14.7 %all_to_all.10 = bf16[16,2,48,128]{3,2,1,0:T(8,128)(2,1)S(1)} all-to-all(bf16[16,2,48,128]{3,2,1,0:T(8,128)(2,1)S(1)} %broadcast_multiply_fusion), channel_id=1, replica_groups=mesh['ep'=16,'tp'=16] {'ep'}, dimensions={0} | all-to-all | bytes 786432 | tf_op jit(solution)/shard_map/all_to_all | solution.py:167
  57.8 1.9 pad_maximum_fusion
  62.5 51.3 %all-gather.5.cloned.1.call-done = bf16[16,2,48,2048]{3,2,0,1:T(8,128)(2,1)} async-done(((bf16[16,2,48,128]{3,2,0,1:T(8,128)(2,1)}), bf16[16,2,48,2048]{3,2,0,1:T(8,128)(2,1)}) %all-gather.5.cloned.1.call-update) | async-done | bytes 6291472 | tf_op jit(solution)/shard_map/all_gather | solution.py:168
  113.8 6.3 %fusion.23 = f32[2,16,48,256]{3,2,1,0:T(8,128)} fusion(bf16[16,2,48,2048]{3,2,0,1:T(8,128)(2,1)} %all-gather.5.cloned.1.call-done, bf16[2,2048,256]{2,1,0:T(8,128)(2,1)} %param.33), kind=kOutput, calls=%fused_computation.40 | convolution fusion | flops 1610612736 | bytes 9961472 | tf_op jit(solution)/shard_map/secd,edf->secf/dot_general | solution.py:169
  120.1 10.0 %convert_bitcast_fusion = bf16[16,2,48,2048]{3,2,0,1:T(8,128)(2,1)} fusion(bf16[2,256,2048]{2,1,0:T(8,128)(2,1)S(1)} %copy-done, f32[2,16,48,256]{3,2,1,0:T(8,128)} %fusion.23, bf16[16,2,48,2048]{3,2,0,1:T(8,128)(2,1)} %all-gather.5.cloned.1.call-done, bf16[2,2048,256]{2,1,0:T(8,128)(2,1)} %param.34), kind=kOutput, calls=%fused_computation.29 | convolution fusion | flops 3226730496 | bytes 18350080 | tf_op jit(solution)/shard_map/secf,efd->secd/dot_general | solution.py:174
  130.1 23.1 %copy.56 = bf16[16,2,48,2048]{2,0,1,3:T(8,128)(2,1)} copy(bf16[16,2,48,2048]{3,2,0,1:T(8,128)(2,1)} %convert_bitcast_fusion) | data formatting | bytes 12582912
  153.2 29.8 %reshape.224 = bf16[2048,1536]{1,0:T(8,128)(2,1)} reshape(bf16[2048,2,16,48]{3,2,1,0:T(8,128)(2,1)} %bitcast.135) | data formatting | bytes 12582912
  183.3 17.5 %all-gather.3.cloned.1.call-done = bf16[8192,544]{1,0:T(8,128)(2,1)} async-done(((bf16[512,544]{1,0:T(8,128)(2,1)}), bf16[8192,544]{1,0:T(8,128)(2,1)}) %all-gather.3.cloned.1.call-update) | async-done | bytes 8912912 | tf_op jit(solution)/shard_map/all_gather | solution.py:14
  200.8 1.6 slice-done
  203.2 7.2 %slice.38 = bf16[8192,512]{1,0:T(8,128)(2,1)} slice(bf16[8192,544]{1,0:T(8,128)(2,1)} %all-gather.3.cloned.1.call-done), slice={[0:8192], [0:512]} | slice | bytes 16777216 | tf_op jit(solution)/shard_map/slice | solution.py:16
  210.4 73.0 %while.15 = (s32[]{:T(128)}, f32[512,2]{0,1:T(2,128)S(1)}, f32[512,2]{0,1:T(2,128)S(1)}, f32[512,2,64]{0,2,1:T(8,128)S(1)}, bf16[16,512,512]{2,1,0:T(8,128)(2,1)...) while((s32[]{:T(128)}, f32[512,2]{0,1:T(2,128)S(1)}, ...), condition=%wide.region_5.6_spmd.clone, body=%wide.region_2.5_spmd.clone.sunk | while | flops 305992704 | bytes 13141125 | solution.py:122
  283.5 3.1 convolution_convert_fusion.2
  286.7 2.1 reshape.225
  288.8 1.8 copy.48
  290.6 5.7 %all-to-all-start.1 = ((bf16[16,2,48,128]{3,2,1,0:T(8,128)(2,1)}), bf16[16,2,48,128]{3,2,1,0:T(8,128)(2,1)S(1)}, u32[]{:S(2)}, u32[]{:S(2)}) async-start(bf16[16,2,48,128]{3,2,1,0:T(8,128)(2,1)} %copy.48), calls=%async_computation.2 | async-start | bytes 786432 | tf_op jit(solution)/shard_map/all_to_all | solution.py:180
  296.5 7.1 %all-to-all-done.1 = bf16[16,2,48,128]{3,2,1,0:T(8,128)(2,1)S(1)} async-done(((bf16[16,2,48,128]{3,2,1,0:T(8,128)(2,1)}), bf16[16,2,48,128]{3,2,1,0:T(8,128)(2,1)S(1)}, u32[]{:S(2)}, u32[]{:S(2)}) %all-to-all-start.1) | async-done | bytes 393248 | tf_op jit(solution)/shard_map/all_to_all | solution.py:180
  303.6 3.2 gather_fusion.1
  306.8 3.5 fusion.37
  310.3 36.6 %reduce-scatter.5.cloned.1.call-done = bf16[32,2048]{1,0:T(8,128)(2,1)} async-done(((bf16[512,2048]{1,0:T(8,128)(2,1)}), bf16[32,2048]{1,0:T(8,128)(2,1)}) %reduce-scatter.5.cloned.1.call-update) | async-done | bytes 131088 | tf_op jit(solution)/shard_map/reduce_scatter | solution.py:136
  (234 shorter events, 83.0 us)
Async XLA Ops:
  7.2 113.0 %copy-start = (bf16[2,256,2048]{2,1,0:T(8,128)(2,1)S(1)}, bf16[2,256,2048]{2,1,0:T(8,128)(2,1)}, u32[]{:S(2)}) copy-start(bf16[2,256,2048]{2,1,0:T(8,128)(2,1)} %param.35) | copy-start | bytes 6291460
  7.2 106.6 %all-gather.5.cloned.1.call-start = ((), (), s32[]{:S(2)}) async-start(), calls=%async_computation.6 | async-start | bytes 6684672 | tf_op jit(solution)/shard_map/all_gather | solution.py:168
  7.2 4.2 %copy-start.2 = (bf16[512,2048]{1,0:T(8,128)(2,1)S(1)}, bf16[512,2048]{1,0:T(8,128)(2,1)}, u32[]{:S(2)}) copy-start(bf16[512,2048]{1,0:T(8,128)(2,1)} %param.29) | copy-start | bytes 6291460
  11.4 0.7 copy-start.11
  39.7 15.9 %copy-start.10 = (bf16[512,32]{0,1:T(8,128)(2,1)S(1)}, bf16[512,32]{0,1:T(8,128)(2,1)}, u32[]{:S(2)}) copy-start(bf16[512,32]{0,1:T(8,128)(2,1)} %param.21) | copy-start | bytes 98308
  39.7 17.7 %copy-start.5 = (bf16[512,512]{1,0:T(8,128)(2,1)S(1)}, bf16[512,512]{1,0:T(8,128)(2,1)}, u32[]{:S(2)}) copy-start(bf16[512,512]{1,0:T(8,128)(2,1)} %param.20) | copy-start | bytes 1572868
  39.7 17.9 %copy-start.13 = (f32[512]{0:T(512)S(1)}, f32[512]{0:T(512)}, u32[]{:S(2)}) copy-start(f32[512]{0:T(512)} %param.23) | copy-start | bytes 6148
  55.5 145.3 %all-gather.3.cloned.1.call-start = ((), (), s32[]{:S(2)}) async-start(), calls=%async_computation.4 | async-start | bytes 11141120 | tf_op jit(solution)/shard_map/all_gather | solution.py:14
  57.6 2.8 copy-start.15
  57.8 2.3 copy-start.6
  59.7 2.1 copy-start.8
  59.7 2.1 copy-start.9
  59.8 226.9 %reduce-scatter.7.cloned.1.call-start = ((), (), s32[]{:S(2)}) async-start(), calls=%async_computation.7 | async-start | bytes 6684672
  60.0 1.9 copy-start.7
  60.0 1.9 copy-start.14
  183.0 163.8 %reduce-scatter.5.cloned.1.call-start = ((), (), s32[]{:S(2)}) async-start(), calls=%async_computation.5 | async-start | bytes 2228224 | tf_op jit(solution)/shard_map/reduce_scatter | solution.py:136
  200.8 1.6 slice-start
  203.2 7.2 %copy-start.3 = (bf16[512,128]{1,0:T(8,128)(2,1)S(1)}, bf16[512,128]{1,0:T(8,128)(2,1)}, u32[]{:S(2)}) copy-start(bf16[512,128]{1,0:T(8,128)(2,1)} %param.26) | copy-start | bytes 393220
  203.2 7.2 %copy-start.4 = (bf16[512,128]{1,0:T(8,128)(2,1)S(1)}, bf16[512,128]{1,0:T(8,128)(2,1)}, u32[]{:S(2)}) copy-start(bf16[512,128]{1,0:T(8,128)(2,1)} %param.27) | copy-start | bytes 393220
  286.6 9.6 %copy-start.12 = (f32[512,2]{0,1:T(2,128)S(1)}, f32[512,2]{0,1:T(2,128)}, u32[]{:S(2)}) copy-start(f32[512,2]{0,1:T(2,128)} %param.32) | copy-start | bytes 12292
  288.8 58.1 %copy-start.1 = (bf16[2,256,2048]{2,1,0:T(8,128)(2,1)S(1)}, bf16[2,256,2048]{2,1,0:T(8,128)(2,1)}, u32[]{:S(2)}) copy-start(bf16[2,256,2048]{2,1,0:T(8,128)(2,1)} %param.35) | copy-start | bytes 6291460
  290.6 13.0 %all-to-all-start.1 = ((bf16[16,2,48,128]{3,2,1,0:T(8,128)(2,1)}), bf16[16,2,48,128]{3,2,1,0:T(8,128)(2,1)S(1)}, u32[]{:S(2)}, u32[]{:S(2)}) async-start(bf16[16,2,48,128]{3,2,1,0:T(8,128)(2,1)} %copy.48), calls=%async_computation.2 | async-start | bytes 786432 | tf_op jit(solution)/shard_map/all_to_all | solution.py:180
Sparse Core Ops, SparseCore 0:
  55.7 58.0 all-gather.4
  116.2 84.5 all-gather.2
  203.4 66.9 reduce-scatter.6
  286.8 60.0 reduce-scatter.4
where the time goes:
time: 356 us; the launch traced here: 353 us
  waiting for transfers between devices  113 us (32%)
  local copies, waits for them, and re-layouts  88.8 us (25%)
  matrix products  88.1 us (25%)
  other arithmetic  27.5 us (8%)
  blocking collectives  14.7 us (4%)
  between operations  14.3 us (4%)
  starting transfers between devices  6.26 us (2%)
    unnamed x38, local copies, waits for them, and re-layouts  56.3 us
    all_gather x1, waiting for transfers between devices, experts(): piece = lax.all_gather(arrived, 'tp', axis=3, tiled=True)  51.3 us
    reduce_scatter x1, waiting for transfers between devices, token_mixer(): lax.psum_scatter(jnp.dot(attended, output_weight, preferred_element_type=...  36.6 us
    dot_general x16, matrix products, scan_step(): jnp.dot(latent_block, value_weight, preferred_element_type=jnp.float32)  21.8 us
    dot_general x16, matrix products, scan_step(): jnp.dot(latent_block, key_weight, preferred_element_type=jnp.float32)  21.7 us
    all_gather x1, waiting for transfers between devices, sent_together(): out, at, outs = (lax.all_gather(both, axis, axis=dim, tiled=True), 0, [])  17.5 us
    all_to_all x1, blocking collectives, experts(): lax.all_to_all(outgoing, 'ep', split_axis=0, concat_axis=0, tiled=True)  14.7 us
    dot_general x1, matrix products, experts(): jnp.einsum('secf,efd->secd', hidden, down_weight, preferred_element_type=...  10 us
  transfers between devices with their start and end apart: 5, of which 4 were waited for; matrix products, arithmetic and copies ran while one was open for 48% of the time, Pallas kernels for 0%

commit v1 on v0

--- a/solution.py
+++ b/solution.py
@@ -165,7 +165,7 @@
         group_count, local_count, capacity, part_width
     )
     arrived = lax.all_to_all(outgoing, "ep", split_axis=0, concat_axis=0, tiled=True)
-    piece = lax.all_gather(arrived, "tp", axis=3, tiled=True)
+    piece = jnp.concatenate(lax.all_gather(arrived, axis_name="tp"), axis=3)
     gate_running = jnp.einsum(
         "secd,edf->secf", piece, gate_weight, preferred_element_type=jnp.float32
     )

time: 356 us -> 349 us (0.980)
  waiting for transfers between devices: 113 us -> 81.6 us
  local copies, waits for them, and re-layouts: 88.8 us -> 111 us
    reshape x0 -> x2, local copies, waits for them, and re-layouts: none -> 23.1 us  [experts(): piece = jnp.concatenate(lax.all_gather(arrived, axis_name='tp'), axis=3)]
    all_gather x1, waiting for transfers between devices: 17.5 us -> 0.02 us  [sent_together(): out, at, outs = (lax.all_gather(both, axis, axis=dim, tiled=True), 0, [])]
    all_gather x1, waiting for transfers between devices: 51.3 us -> 40.4 us  [experts(): piece = jnp.concatenate(lax.all_gather(arrived, axis_name='tp'), axis=3)]
  transfers between devices with their start and end apart: 5 -> 5, of which waited for: 4 -> 3; matrix products, arithmetic and copies ran while one was open for 48% -> 56% of each run, Pallas kernels for 0% -> 0%
where the time goes in v1:
time: 349 us; the launch traced here: 346 us
  local copies, waits for them, and re-layouts  111 us (32%)
  matrix products  88.2 us (25%)
  waiting for transfers between devices  81.6 us (23%)
  other arithmetic  27.5 us (8%)
  blocking collectives  14.8 us (4%)
  between operations  14.3 us (4%)
  starting transfers between devices  7.53 us (2%)
    unnamed x38, local copies, waits for them, and re-layouts  56.3 us
    all_gather x1, waiting for transfers between devices, experts(): piece = jnp.concatenate(lax.all_gather(arrived, axis_name='tp'), axis=3)  40.4 us
    reduce_scatter x1, waiting for transfers between devices, token_mixer(): lax.psum_scatter(jnp.dot(attended, output_weight, preferred_element_type=...  33.4 us
    reshape x2, local copies, waits for them, and re-layouts, experts(): piece = jnp.concatenate(lax.all_gather(arrived, axis_name='tp'), axis=3)  23.1 us
    dot_general x16, matrix products, scan_step(): jnp.dot(latent_block, key_weight, preferred_element_type=jnp.float32)  21.8 us
    dot_general x16, matrix products, scan_step(): jnp.dot(latent_block, value_weight, preferred_element_type=jnp.float32)  21.7 us
    all_to_all x1, blocking collectives, experts(): lax.all_to_all(outgoing, 'ep', split_axis=0, concat_axis=0, tiled=True)  14.8 us
    dot_general x1, matrix products, experts(): jnp.einsum('secf,efd->secd', hidden, down_weight, preferred_element_type=...  10 us
  transfers between devices with their start and end apart: 5, of which 3 were waited for; matrix products, arithmetic and copies ran while one was open for 56% of the time, Pallas kernels for 0%

profile of v1, /device:TPU:6, one launch (start us, length us, event | category | flops | bytes accessed | tf_op | source)
XLA Modules:
  0.0 346.2 jit_solution(7110002154780229827)
XLA Ops:
  7.2 4.2 %convert_element_type.83 = f32[512,2048]{1,0:T(8,128)} convert(bf16[512,2048]{1,0:T(8,128)(2,1)} %param.29) | non-fusion elementwise | flops 1048576 | bytes 6291456 | tf_op jit(solution)/shard_map/convert_element_type | solution.py:22
  12.7 9.0 %reduce-window.6 = s32[32,8,128]{2,1,0:T(8,128)S(1)} reduce-window(s32[32,8,128]{2,1,0:T(8,128)S(1)} %fusion.46, s32[]{:T(128)} %constant.30.clone.1), window={size=1x1x128 pad=0_0x0_0x127_0}, to_apply=%region_8.9 | reduce-window | flops 4161536 | bytes 262148 | tf_op jit(solution)/shard_map/reduce-window
  22.6 4.3 %scatter_custom_fusion = s32[1536]{0:T(1024)S(1)} fusion(s32[1024]{0:T(1024)S(1)} %bitcast.158, s32[1024]{0:T(1024)S(1)} %add_select_fusion, s32[]{:T(128)} %constant.30.clone.1), kind=kCustom, calls=%fused_computation.89 | custom fusion | bytes 6148 | tf_op jit(solution)/shard_map/scatter | solution.py:160
  26.9 7.6 %scatter_custom_fusion.1 = bf16[1536]{0:T(1024)(128)(2,1)S(1)} fusion(s32[1024]{0:T(1024)S(1)} %bitcast.159, bf16[1024]{0:T(1024)(128)(2,1)S(1)} %broadcast.163, bf16[]{:T(256)} %constant.82.clone.1), kind=kCustom, calls=%fused_computation.93 | custom fusion | bytes 3074 | tf_op jit(solution)/shard_map/scatter | solution.py:161
  36.5 3.2 gather_fusion
  40.0 14.8 %all_to_all.10 = bf16[16,2,48,128]{3,2,1,0:T(8,128)(2,1)} all-to-all(bf16[16,2,48,128]{3,2,1,0:T(8,128)(2,1)S(1)} %broadcast_multiply_fusion), channel_id=1, replica_groups=mesh['ep'=16,'tp'=16] {'ep'}, dimensions={0} | all-to-all | bytes 786432 | tf_op jit(solution)/shard_map/all_to_all | solution.py:167
  57.1 1.9 pad_maximum_fusion
  61.8 40.4 %all-gather.6.cloned.1.call-done = bf16[256,2,48,128]{3,2,1,0:T(8,128)(2,1)} async-done(((bf16[16,2,48,128]{3,2,1,0:T(8,128)(2,1)}), bf16[256,2,48,128]{3,2,1,0:T(8,128)(2,1)}) %all-gather.6.cloned.1.call-update) | async-done | bytes 6291472 | tf_op jit(solution)/shard_map/all_gather | solution.py:168
  102.2 12.7 %copy.46 = bf16[16,2,48,16,128]{4,3,2,0,1:T(8,128)(2,1)} copy(bf16[16,2,48,16,128]{4,2,1,0,3:T(8,128)(2,1)} %bitcast.148) | data formatting | bytes 12582912 | tf_op jit(solution)/shard_map/reshape | solution.py:168
  114.9 10.4 %reshape.190 = bf16[16,2,48,2048]{3,2,0,1:T(8,128)(2,1)} reshape(bf16[16,2,48,16,128]{4,3,2,0,1:T(8,128)(2,1)} %copy.46) | data formatting | bytes 12582912 | tf_op jit(solution)/shard_map/reshape | solution.py:168
  125.4 6.5 %fusion.23 = f32[2,16,48,256]{3,2,1,0:T(8,128)} fusion(bf16[16,2,48,2048]{3,2,0,1:T(8,128)(2,1)} %reshape.190, bf16[2,2048,256]{2,1,0:T(8,128)(2,1)} %param.33), kind=kOutput, calls=%fused_computation.40 | convolution fusion | flops 1610612736 | bytes 9961472 | tf_op jit(solution)/shard_map/secd,edf->secf/dot_general | solution.py:169
  131.9 10.0 %convert_bitcast_fusion = bf16[16,2,48,2048]{3,2,0,1:T(8,128)(2,1)} fusion(bf16[2,256,2048]{2,1,0:T(8,128)(2,1)S(1)} %copy-done, f32[2,16,48,256]{3,2,1,0:T(8,128)} %fusion.23, bf16[16,2,48,2048]{3,2,0,1:T(8,128)(2,1)} %reshape.190, bf16[2,2048,256]{2,1,0:T(8,128)(2,1)} %param.34), kind=kOutput, calls=%fused_computation.29 | convolution fusion | flops 3226730496 | bytes 18350080 | tf_op jit(solution)/shard_map/secf,efd->secd/dot_general | solution.py:174
  141.9 23.1 %copy.55 = bf16[16,2,48,2048]{2,0,1,3:T(8,128)(2,1)} copy(bf16[16,2,48,2048]{3,2,0,1:T(8,128)(2,1)} %convert_bitcast_fusion) | data formatting | bytes 12582912
  164.9 29.7 %reshape.233 = bf16[2048,1536]{1,0:T(8,128)(2,1)} reshape(bf16[2048,2,16,48]{3,2,1,0:T(8,128)(2,1)} %bitcast.142) | data formatting | bytes 12582912
  197.2 7.2 %slice.38 = bf16[8192,512]{1,0:T(8,128)(2,1)} slice(bf16[8192,544]{1,0:T(8,128)(2,1)} %all-gather.4.cloned.1.call-done), slice={[0:8192], [0:512]} | slice | bytes 16777216 | tf_op jit(solution)/shard_map/slice | solution.py:16
  204.3 73.1 %while.15 = (s32[]{:T(128)}, f32[512,2]{0,1:T(2,128)S(1)}, f32[512,2]{0,1:T(2,128)S(1)}, f32[512,2,64]{0,2,1:T(8,128)S(1)}, bf16[16,512,512]{2,1,0:T(8,128)(2,1)...) while((s32[]{:T(128)}, f32[512,2]{0,1:T(2,128)S(1)}, ...), condition=%wide.region_5.6_spmd.clone, body=%wide.region_2.5_spmd.clone.sunk | while | flops 305992704 | bytes 13141125 | solution.py:122
  277.4 3.1 convolution_convert_fusion.2
  280.6 2.1 reshape.234
  282.7 1.8 copy.47
  284.5 7.2 %all-to-all-start.1 = ((bf16[16,2,48,128]{3,2,1,0:T(8,128)(2,1)}), bf16[16,2,48,128]{3,2,1,0:T(8,128)(2,1)S(1)}, u32[]{:S(2)}, u32[]{:S(2)}) async-start(bf16[16,2,48,128]{3,2,1,0:T(8,128)(2,1)} %copy.47), calls=%async_computation.2 | async-start | bytes 786432 | tf_op jit(solution)/shard_map/all_to_all | solution.py:180
  291.9 7.7 %all-to-all-done.1 = bf16[16,2,48,128]{3,2,1,0:T(8,128)(2,1)S(1)} async-done(((bf16[16,2,48,128]{3,2,1,0:T(8,128)(2,1)}), bf16[16,2,48,128]{3,2,1,0:T(8,128)(2,1)S(1)}, u32[]{:S(2)}, u32[]{:S(2)}) %all-to-all-start.1) | async-done | bytes 393248 | tf_op jit(solution)/shard_map/all_to_all | solution.py:180
  299.6 3.2 gather_fusion.1
  302.8 3.5 fusion.37
  306.2 33.4 %reduce-scatter.5.cloned.1.call-done = bf16[32,2048]{1,0:T(8,128)(2,1)} async-done(((bf16[512,2048]{1,0:T(8,128)(2,1)}), bf16[32,2048]{1,0:T(8,128)(2,1)}) %reduce-scatter.5.cloned.1.call-update) | async-done | bytes 131088 | tf_op jit(solution)/shard_map/reduce_scatter | solution.py:136
  (235 shorter events, 83.6 us)
Async XLA Ops:
  7.2 124.7 %copy-start = (bf16[2,256,2048]{2,1,0:T(8,128)(2,1)S(1)}, bf16[2,256,2048]{2,1,0:T(8,128)(2,1)}, u32[]{:S(2)}) copy-start(bf16[2,256,2048]{2,1,0:T(8,128)(2,1)} %param.35) | copy-start | bytes 6291460
  7.2 95.0 %all-gather.6.cloned.1.call-start = ((), (), s32[]{:S(2)}) async-start(), calls=%async_computation.6 | async-start | bytes 6684672 | tf_op jit(solution)/shard_map/all_gather | solution.py:168
  7.2 4.2 %copy-start.2 = (bf16[512,2048]{1,0:T(8,128)(2,1)S(1)}, bf16[512,2048]{1,0:T(8,128)(2,1)}, u32[]{:S(2)}) copy-start(bf16[512,2048]{1,0:T(8,128)(2,1)} %param.29) | copy-start | bytes 6291460
  11.4 0.7 copy-start.11
  36.5 18.4 %copy-start.10 = (bf16[512,32]{0,1:T(8,128)(2,1)S(1)}, bf16[512,32]{0,1:T(8,128)(2,1)}, u32[]{:S(2)}) copy-start(bf16[512,32]{0,1:T(8,128)(2,1)} %param.21) | copy-start | bytes 98308
  39.7 17.0 %copy-start.5 = (bf16[512,512]{1,0:T(8,128)(2,1)S(1)}, bf16[512,512]{1,0:T(8,128)(2,1)}, u32[]{:S(2)}) copy-start(bf16[512,512]{1,0:T(8,128)(2,1)} %param.20) | copy-start | bytes 1572868
  39.7 17.2 %copy-start.13 = (f32[512]{0:T(512)S(1)}, f32[512]{0:T(512)}, u32[]{:S(2)}) copy-start(f32[512]{0:T(512)} %param.23) | copy-start | bytes 6148
  54.8 139.9 %all-gather.4.cloned.1.call-start = ((), (), s32[]{:S(2)}) async-start(), calls=%async_computation.4 | async-start | bytes 11141120 | tf_op jit(solution)/shard_map/all_gather | solution.py:14
  56.9 2.8 copy-start.15
  57.1 2.2 copy-start.6
  59.0 2.1 copy-start.8
  59.0 2.1 copy-start.9
  59.1 221.5 %reduce-scatter.7.cloned.1.call-start = ((), (), s32[]{:S(2)}) async-start(), calls=%async_computation.7 | async-start | bytes 6684672
  59.3 1.9 copy-start.7
  59.3 1.9 copy-start.14
  194.7 145.0 %reduce-scatter.5.cloned.1.call-start = ((), (), s32[]{:S(2)}) async-start(), calls=%async_computation.5 | async-start | bytes 2228224 | tf_op jit(solution)/shard_map/reduce_scatter | solution.py:136
  194.7 1.6 slice-start
  197.1 7.2 %copy-start.3 = (bf16[512,128]{1,0:T(8,128)(2,1)S(1)}, bf16[512,128]{1,0:T(8,128)(2,1)}, u32[]{:S(2)}) copy-start(bf16[512,128]{1,0:T(8,128)(2,1)} %param.26) | copy-start | bytes 393220
  197.1 7.2 %copy-start.4 = (bf16[512,128]{1,0:T(8,128)(2,1)S(1)}, bf16[512,128]{1,0:T(8,128)(2,1)}, u32[]{:S(2)}) copy-start(bf16[512,128]{1,0:T(8,128)(2,1)} %param.27) | copy-start | bytes 393220
  280.6 11.1 %copy-start.12 = (f32[512,2]{0,1:T(2,128)S(1)}, f32[512,2]{0,1:T(2,128)}, u32[]{:S(2)}) copy-start(f32[512,2]{0,1:T(2,128)} %param.32) | copy-start | bytes 12292
  282.7 56.9 %copy-start.1 = (bf16[2,256,2048]{2,1,0:T(8,128)(2,1)S(1)}, bf16[2,256,2048]{2,1,0:T(8,128)(2,1)}, u32[]{:S(2)}) copy-start(bf16[2,256,2048]{2,1,0:T(8,128)(2,1)} %param.35) | copy-start | bytes 6291460
  284.5 15.0 %all-to-all-start.1 = ((bf16[16,2,48,128]{3,2,1,0:T(8,128)(2,1)}), bf16[16,2,48,128]{3,2,1,0:T(8,128)(2,1)S(1)}, u32[]{:S(2)}, u32[]{:S(2)}) async-start(bf16[16,2,48,128]{3,2,1,0:T(8,128)(2,1)} %copy.47), calls=%async_computation.2 | async-start | bytes 786432 | tf_op jit(solution)/shard_map/all_to_all | solution.py:180
Sparse Core Ops, SparseCore 0:
  55.0 47.2 all-gather.5
  104.6 84.0 all-gather.3
  194.8 65.9 reduce-scatter.6
  280.7 58.9 reduce-scatter.4
